TPU v7x, 512 devices: a whole 4x8x8 slice. The times are simulated.
512 devices in a mesh: ep: 128 (over z, y, core), tp: 4 (over x).
Axes of the slice: x: 4, y: 8, z: 8, core: 2. Of those that a mesh axis runs over, the one named last changes fastest.
Arguments:
- residual_in: bfloat16 [2560, 1024], P('ep', 'tp'), may hold values from -64 to 64
- queries: bfloat16 [2560, 512], P(('ep', 'tp')), may hold values from -6 to 6
- cache_keys: bfloat16 [2560, 1024, 128], P(('ep', 'tp')), may hold values from -6 to 6
- cache_values: bfloat16 [2560, 1024, 128], P(('ep', 'tp')), may hold values from -24 to 24
- lengths: int32 [2560], P(('ep', 'tp')), may hold values from 256 to 1024
- stick_offset: float32 [8], replicated, may hold values from 0.5 to 6
- out_weight: bfloat16 [512, 1024], P(None, 'tp'), may hold values from -0.25 to 0.25
- norm1_gain: float32 [1024], P('tp'), may hold values from 0.3 to 3.1
- norm1_bias: float32 [1024], P('tp'), may hold values from -1.5 to 1.5
- routes: int32 [2560, 6], P('ep'), may hold values from 0 to 127, all different within a row; in each aligned block of 20 rows (0 to 19, 20 to 39, ...) at most 2 rows name the same one
- route_weights: float32 [2560, 6], P('ep'), may hold values from 0.1 to 0.8
- expert_gate: bfloat16 [128, 1024, 512], P('ep', None, 'tp'), may hold values from -0.1875 to 0.1875
- expert_up: bfloat16 [128, 1024, 512], P('ep', None, 'tp'), may hold values from -0.1875 to 0.1875
- expert_down: bfloat16 [128, 512, 1024], P('ep', 'tp'), may hold values from -0.25 to 0.25
- shared_gate: bfloat16 [1024, 512], P(None, 'tp'), may hold values from -0.1875 to 0.1875
- shared_up: bfloat16 [1024, 512], P(None, 'tp'), may hold values from -0.1875 to 0.1875
- shared_down: bfloat16 [512, 1024], P('tp'), may hold values from -0.25 to 0.25
- norm2_gain: float32 [1024], P('tp'), may hold values from 0.1 to 1.9
- norm2_bias: float32 [1024], P('tp'), may hold values from -1.5 to 1.5
Outputs:
- layer_out: bfloat16 [2560, 1024], P('ep', 'tp')
Inputs may be any that keep to these rules, and one draw needn't show every extreme that they name: `routes`: each row names 6 different experts; among the rows of one index of ep no expert is named more than 2 times.
All inputs are finite; a program needn't handle non-finite values.
Results may differ from a plain program's by a relative error of at most 0.0095.
Values may be sent and summed in bfloat16 or wider, within the bound.
No kernel may reach another device: no remote copies, remote signals or barrier semaphores. Data moves between devices by JAX's collectives and lax.ppermute only.
A program may use at most 64 MiB of HBM per device.

v0:
```python
import jax
import jax.numpy as jnp
from jax import lax
from jax.sharding import PartitionSpec as P

H = 8
HD = 64
KVH = 2
CACHE = 1024
TOPK = 6
RESIDUAL_SCALE = 2.0**0.25
EPSILON = 1e-05


def joined_along(blocks, dim):
    blocks = jnp.moveaxis(blocks, 0, dim)
    shape = blocks.shape
    return blocks.reshape(*shape[:dim], shape[dim] * shape[dim + 1], *shape[dim + 2 :])


def from_everyone(value, axis):
    copies = jnp.broadcast_to(value, (lax.axis_size(axis), *value.shape))
    return lax.all_to_all(copies, axis, split_axis=0, concat_axis=0, tiled=True)


def gathered_copies(value, axis, dim):
    return joined_along(from_everyone(value, axis), dim)


def rows_first(arrays, axis, dims):
    turned = [jnp.moveaxis(a, dim, 0) for a, dim in zip(arrays, dims)]
    both = jnp.concatenate([t.reshape(len(t), -1) for t in turned], axis=1)
    out, at, done = (lax.all_gather(both, axis, axis=0, tiled=True), 0, [])
    for t, dim in zip(turned, dims):
        piece = out[:, at : at + t[0].size].reshape(-1, *t.shape[1:])
        done.append(jnp.moveaxis(piece, 0, dim))
        at += t[0].size
    return tuple(done)


def cut_along(value, dim, devices):
    before, after = (value.shape[:dim], value.shape[dim + 1 :])
    return jnp.moveaxis(value.reshape(*before, devices, -1, *after), dim, 0)


def sent_and_summed(value, axis, dim):
    blocks = cut_along(value, dim, lax.axis_size(axis))
    arrived = lax.all_to_all(blocks, axis, split_axis=0, concat_axis=0, tiled=True)
    return arrived.astype(jnp.float32).sum(axis=0)


def over_copies(value, axis):
    everything = from_everyone(value, axis)
    return jnp.sum(everything, axis=0)


def packed_total(arrays, axis):
    ends = [0]
    for a in arrays:
        ends.append(ends[-1] + a.size)
    running = over_copies(jnp.concatenate([a.ravel() for a in arrays]), axis)
    return tuple((running[b:e].reshape(a.shape) for a, b, e in zip(arrays, ends, ends[1:])))


def normalize(totals, squares, entries, values, scales, shifts):
    centre = totals / entries
    spread = squares / entries - centre * centre
    return (values - centre) * lax.rsqrt(spread + EPSILON) * scales + shifts


def stick_read(queries, keys_block, values_block, lengths, offsets):
    seq_count = queries.shape[0]
    grouped = H // KVH
    query_heads = queries.reshape(seq_count, KVH, grouped, HD)
    key_heads = keys_block.reshape(seq_count, CACHE, KVH, HD)
    value_heads = values_block.reshape(seq_count, CACHE, KVH, HD)
    scores = jnp.einsum(
        "sgjd,slgd->sgjl", query_heads, key_heads, preferred_element_type=jnp.float32
    )
    scores = scores * HD ** (-0.5) - offsets.reshape(1, KVH, grouped, 1)
    live_mask = (jnp.arange(CACHE)[None, :] < lengths[:, None])[:, None, None, :]
    keep_log = jnp.where(live_mask, jax.nn.log_sigmoid(-scores), 0.0)
    after_log = lax.cumsum(keep_log, axis=3, reverse=True) - keep_log
    weights = jnp.where(live_mask, jnp.exp(jax.nn.log_sigmoid(scores) + after_log), 0.0)
    weights = weights.astype(jnp.bfloat16)
    mixed = jnp.einsum("sgjl,slgd->sgjd", weights, value_heads, preferred_element_type=jnp.float32)
    return mixed.reshape(seq_count, H * HD).astype(jnp.bfloat16)


def body(
    residual_in,
    queries,
    cache_keys,
    cache_values,
    lengths,
    stick_offset,
    out_weight,
    norm1_gain,
    norm1_bias,
    routes,
    route_weights,
    expert_gate,
    expert_up,
    expert_down,
    shared_gate,
    shared_up,
    shared_down,
    norm2_gain,
    norm2_bias,
):
    mixed = stick_read(queries, cache_keys, cache_values, lengths, stick_offset)
    attended = jnp.dot(
        gathered_copies(mixed, "tp", 0), out_weight, preferred_element_type=jnp.float32
    )
    before = RESIDUAL_SCALE * residual_in.astype(jnp.float32) + attended
    group_rows, columns = residual_in.shape
    full_width = columns * lax.axis_size("tp")
    widened, scales, shifts = rows_first((before, norm1_gain, norm1_bias), "tp", (1, 0, 0))
    whole = normalize(
        jnp.sum(widened, axis=1, keepdims=True),
        jnp.sum(widened * widened, axis=1, keepdims=True),
        full_width,
        widened,
        scales,
        shifts,
    ).astype(jnp.bfloat16)
    normed = lax.dynamic_slice_in_dim(whole, lax.axis_index("tp") * columns, columns, 1)
    experts = lax.axis_size("ep")
    capacity = min(group_rows, 2 * ((group_rows * TOPK + experts - 1) // experts))
    slots_all = experts * capacity
    chosen = routes.reshape(-1)
    order_ids = jnp.arange(chosen.shape[0])
    matches = (chosen[:, None] == chosen[None, :]) & (order_ids[None, :] < order_ids[:, None])
    targets = chosen * capacity + jnp.sum(matches.astype(jnp.int32), axis=1)
    picks = (targets[:, None] == jnp.arange(slots_all)[None, :]).astype(jnp.float32)
    picks = picks.reshape(group_rows, TOPK, slots_all)
    dispatch = jnp.sum(picks, axis=1).astype(jnp.bfloat16)
    combine = jnp.sum(picks * route_weights[:, :, None], axis=1)
    parcel = jnp.einsum("sr,sd->rd", dispatch, whole, preferred_element_type=jnp.float32)
    parcel = parcel.astype(jnp.bfloat16).reshape(experts, capacity, full_width)
    arrived = lax.all_to_all(parcel, "ep", split_axis=0, concat_axis=0, tiled=True)
    gate_part = jnp.einsum(
        "ecd,df->ecf", arrived, expert_gate[0], preferred_element_type=jnp.float32
    )
    up_part = jnp.einsum("ecd,df->ecf", arrived, expert_up[0], preferred_element_type=jnp.float32)
    hidden = (jax.nn.silu(gate_part) * up_part).astype(jnp.bfloat16)
    partial_value = jnp.einsum(
        "ecf,fd->ecd", hidden, expert_down[0], preferred_element_type=jnp.float32
    )
    summed = sent_and_summed(partial_value.astype(jnp.bfloat16), "tp", 2).astype(jnp.bfloat16)
    returned = lax.all_to_all(summed, "ep", split_axis=0, concat_axis=0, tiled=True)
    routed = jnp.dot(
        combine,
        returned.reshape(slots_all, columns).astype(jnp.float32),
        precision=lax.Precision.HIGHEST,
    )
    shared_hidden = (
        jax.nn.silu(jnp.dot(whole, shared_gate, preferred_element_type=jnp.float32))
        * jnp.dot(whole, shared_up, preferred_element_type=jnp.float32)
    ).astype(jnp.bfloat16)
    shared_term = jnp.dot(shared_hidden, shared_down, preferred_element_type=jnp.float32)
    shared = sent_and_summed(shared_term.astype(jnp.bfloat16), "tp", 1)
    after = RESIDUAL_SCALE * normed.astype(jnp.float32) + routed + shared
    final_totals, final_squares = packed_total(
        (jnp.sum(after, axis=1), jnp.sum(after * after, axis=1)), "tp"
    )
    return normalize(
        final_totals[:, None], final_squares[:, None], full_width, after, norm2_gain, norm2_bias
    ).astype(jnp.bfloat16)


def solution(mesh):
    in_specs = (
        P("ep", "tp"),
        P(("ep", "tp"), None),
        P(("ep", "tp"), None, None),
        P(("ep", "tp"), None, None),
        P(("ep", "tp")),
        P(),
        P(None, "tp"),
        P("tp"),
        P("tp"),
        P("ep", None),
        P("ep", None),
        P("ep", None, "tp"),
        P("ep", None, "tp"),
        P("ep", "tp", None),
        P(None, "tp"),
        P(None, "tp"),
        P("tp", None),
        P("tp"),
        P("tp"),
    )
    out_specs = P("ep", "tp")
    return jax.shard_map(body, mesh=mesh, in_specs=in_specs, out_specs=out_specs, check_vma=False)
```

profile of v0, /device:TPU:1, one launch (start us, length us, event | category | flops | bytes accessed | tf_op | source)
XLA Modules:
  0.0 168.4 jit_solution(15376619532127802602)
XLA Ops:
  0.0 0.8 iota_compare_fusion.2
  0.8 1.6 copy.87
  2.6 0.4 fusion.19
  3.1 49.5 %reduce-window.6 = f32[5,2,4,8,128]{4,3,2,1,0:T(8,128)S(1)} reduce-window(f32[5,2,4,8,128]{4,3,2,1,0:T(8,128)S(1)} %reshape.118, f32[]{:T(128)} %constant.30.clone.1), window={size=1x1x1x1x128 pad=0_0x0_0x0_0x0_0x0_127}, to_apply=%region_0.1 | reduce-window | flops 5201920 | bytes 327684 | tf_op jit(solution)/shard_map/reduce-window
  52.7 1.8 %reduce-window.9 = f32[5,2,4,9]{3,2,1,0:T(4,128)S(1)} reduce-window(f32[5,2,4,8]{3,2,1,0:T(4,128)S(1)} %slice_reduce_fusion, f32[]{:T(128)} %constant.30.clone.1), window={size=1x1x1x8 pad=0_0x0_0x0_0x0_8}, to_apply=%region_1.2 | reduce-window | flops 2520 | bytes 2724 | tf_op jit(solution)/shard_map/reduce-window.1
  54.8 0.6 copy.88
  55.5 0.6 convolution_convert_fusion.3
  56.2 0.6 broadcast_in_dim.19
  56.8 4.8 %all-to-all-start = ((bf16[4,5,512]{2,1,0:T(8,128)(2,1)}), bf16[4,5,512]{2,1,0:T(8,128)(2,1)S(1)}, u32[]{:S(2)}, u32[]{:S(2)}) async-start(bf16[4,5,512]{2,1,0:T(8,128)(2,1)} %broadcast_in_dim.19), calls=%async_computation | async-start | bytes 65536 | tf_op jit(solution)/shard_map/all_to_all | solution.py:23
  61.8 0.2 convert_reduce_fusion.2
  62.3 3.6 %all-to-all-done = bf16[4,5,512]{2,1,0:T(8,128)(2,1)S(1)} async-done(((bf16[4,5,512]{2,1,0:T(8,128)(2,1)}), bf16[4,5,512]{2,1,0:T(8,128)(2,1)S(1)}, u32[]{:S(2)}, u32[]{:S(2)}) %all-to-all-start) | async-done | bytes 20512 | tf_op jit(solution)/shard_map/all_to_all | solution.py:23
  66.0 0.2 fusion.3
  66.2 9.0 %all_gather.3 = f32[1024,22]{0,1:T(8,128)S(1)} all-gather(f32[256,22]{0,1:T(8,128)S(1)} %pad_maximum_fusion), channel_id=1, replica_groups=mesh['ep'=128,'tp'=4] {'tp'}, dimensions={0}, use_global_device_ids=true | all-gather | bytes 112640 | tf_op jit(solution)/shard_map/all_gather | solution.py:33
  75.5 0.3 convolution_convert_fusion.1
  75.8 0.2 reshape.124
  76.0 42.3 %all_to_all.31 = bf16[128,2,1024]{2,1,0:T(2,128)(2,1)S(1)} all-to-all(bf16[128,2,1024]{2,1,0:T(2,128)(2,1)S(1)} %reshape.124), channel_id=1, replica_groups=mesh['ep'=128,'tp'=4] {'ep'}, dimensions={0} | all-to-all | bytes 1048576 | tf_op jit(solution)/shard_map/all_to_all | solution.py:141
  118.3 0.3 fusion.7
  118.6 0.5 convolution_convert_fusion
  119.2 0.8 copy.107
  120.0 3.5 %all-to-all-start.2 = ((bf16[4,128,2,256]{3,1,2,0:T(8,128)(2,1)}), bf16[4,128,2,256]{3,1,2,0:T(8,128)(2,1)S(1)}, u32[]{:S(2)}, u32[]{:S(2)}) async-start(bf16[4,128,2,256]{3,1,2,0:T(8,128)(2,1)} %bitcast.48), calls=%async_computation.2 | async-start | bytes 1048576 | tf_op jit(solution)/shard_map/all_to_all | solution.py:48
  123.5 0.2 fusion.43
  123.7 0.3 convolution_convert_fusion.2
  124.0 0.6 copy.108
  124.6 8.6 %all-to-all-done.2 = bf16[4,128,2,256]{3,1,2,0:T(8,128)(2,1)S(1)} async-done(((bf16[4,128,2,256]{3,1,2,0:T(8,128)(2,1)}), bf16[4,128,2,256]{3,1,2,0:T(8,128)(2,1)S(1)}, u32[]{:S(2)}, u32[]{:S(2)}) %all-to-all-start.2) | async-done | bytes 524320 | tf_op jit(solution)/shard_map/all_to_all | solution.py:48
  133.3 3.3 %all-to-all-start.4 = ((bf16[4,20,256]{2,1,0:T(8,128)(2,1)}), bf16[4,20,256]{2,1,0:T(8,128)(2,1)S(1)}, u32[]{:S(2)}, u32[]{:S(2)}) async-start(bf16[4,20,256]{2,1,0:T(8,128)(2,1)} %bitcast.49), calls=%async_computation.4 | async-start | bytes 98304 | tf_op jit(solution)/shard_map/all_to_all | solution.py:48
  136.6 0.8 copy.95
  137.4 3.5 %all-to-all-done.4 = bf16[4,20,256]{2,1,0:T(8,128)(2,1)S(1)} async-done(((bf16[4,20,256]{2,1,0:T(8,128)(2,1)}), bf16[4,20,256]{2,1,0:T(8,128)(2,1)S(1)}, u32[]{:S(2)}, u32[]{:S(2)}) %all-to-all-start.4) | async-done | bytes 40992 | tf_op jit(solution)/shard_map/all_to_all | solution.py:48
  140.9 6.9 %all-to-all-start.3 = ((bf16[128,2,256]{2,1,0:T(2,128)(2,1)}), bf16[128,2,256]{2,1,0:T(2,128)(2,1)S(1)}, u32[]{:S(2)}, u32[]{:S(2)}) async-start(bf16[128,2,256]{2,1,0:T(2,128)(2,1)} %copy.95), calls=%async_computation.3 | async-start | bytes 262144 | tf_op jit(solution)/shard_map/all_to_all | solution.py:151
  147.9 12.8 %all-to-all-done.3 = bf16[128,2,256]{2,1,0:T(2,128)(2,1)S(1)} async-done(((bf16[128,2,256]{2,1,0:T(2,128)(2,1)}), bf16[128,2,256]{2,1,0:T(2,128)(2,1)S(1)}, u32[]{:S(2)}, u32[]{:S(2)}) %all-to-all-start.3) | async-done | bytes 131104 | tf_op jit(solution)/shard_map/all_to_all | solution.py:151
  160.7 0.3 fusion.41
  161.1 6.5 %all_to_all.32 = f32[4,1,40]{2,1,0:T(1,128)S(1)} all-to-all(f32[4,1,40]{2,1,0:T(1,128)S(1)} %broadcast_in_dim.20), channel_id=1, replica_groups=mesh['ep'=128,'tp'=4] {'tp'}, dimensions={0} | all-to-all | bytes 1280 | tf_op jit(solution)/shard_map/all_to_all | solution.py:23
  167.7 0.7 add_convert_fusion.1
  (62 shorter events, 1.9 us)
Async XLA Ops:
  0.0 118.6 %copy-start = (bf16[1,128,1024]{2,1,0:T(8,128)(2,1)S(1)}, bf16[1,128,1024]{2,1,0:T(8,128)(2,1)}, u32[]{:S(2)}) copy-start(bf16[1,128,1024]{2,1,0:T(8,128)(2,1)} %param.32) | copy-start | bytes 786436
  0.8 1.6 copy-start.8
  0.8 1.7 %copy-start.16 = (f32[8]{0:T(128)S(1)}, f32[8]{0:T(128)}, u32[]{:S(2)}) copy-start(f32[8]{0:T(128)} %param.24) | copy-start | bytes 100
  2.6 52.2 %copy-start.1 = (bf16[5,1024,128]{2,1,0:T(8,128)(2,1)S(1)}, bf16[5,1024,128]{2,1,0:T(8,128)(2,1)}, u32[]{:S(2)}) copy-start(bf16[5,1024,128]{2,1,0:T(8,128)(2,1)} %param.22) | copy-start | bytes 3932164
  55.4 6.2 %copy-start.6 = (s32[20,6]{0,1:T(8,128)S(1)}, s32[20,6]{0,1:T(8,128)}, u32[]{:S(2)}) copy-start(s32[20,6]{0,1:T(8,128)} %param.28) | copy-start | bytes 1444
  55.4 6.8 %copy-start.9 = (f32[20,6]{0,1:T(8,128)S(1)}, f32[20,6]{0,1:T(8,128)}, u32[]{:S(2)}) copy-start(f32[20,6]{0,1:T(8,128)} %param.29) | copy-start | bytes 1444
  55.4 10.5 %copy-start.2 = (bf16[512,256]{1,0:T(8,128)(2,1)S(1)}, bf16[512,256]{1,0:T(8,128)(2,1)}, u32[]{:S(2)}) copy-start(bf16[512,256]{1,0:T(8,128)(2,1)} %param.25) | copy-start | bytes 786436
  55.5 10.5 %copy-start.7 = (bf16[20,256]{1,0:T(8,128)(2,1)S(1)}, bf16[20,256]{1,0:T(8,128)(2,1)}, u32[]{:S(2)}) copy-start(bf16[20,256]{1,0:T(8,128)(2,1)} %param.19) | copy-start | bytes 30724
  55.5 10.7 %copy-start.10 = (f32[256]{0:T(256)S(1)}, f32[256]{0:T(256)}, u32[]{:S(2)}) copy-start(f32[256]{0:T(256)} %param.27) | copy-start | bytes 3076
  55.5 10.7 %copy-start.11 = (f32[256]{0:T(256)S(1)}, f32[256]{0:T(256)}, u32[]{:S(2)}) copy-start(f32[256]{0:T(256)} %param.26) | copy-start | bytes 3076
  56.8 9.1 %all-to-all-start = ((bf16[4,5,512]{2,1,0:T(8,128)(2,1)}), bf16[4,5,512]{2,1,0:T(8,128)(2,1)S(1)}, u32[]{:S(2)}, u32[]{:S(2)}) async-start(bf16[4,5,512]{2,1,0:T(8,128)(2,1)} %broadcast_in_dim.19), calls=%async_computation | async-start | bytes 65536 | tf_op jit(solution)/shard_map/all_to_all | solution.py:23
  75.5 42.8 %copy-start.14 = (bf16[1,1024,128]{2,1,0:T(8,128)(2,1)S(1)}, bf16[1,1024,128]{2,1,0:T(8,128)(2,1)}, u32[]{:S(2)}) copy-start(bf16[1,1024,128]{2,1,0:T(8,128)(2,1)} %param.30) | copy-start | bytes 786436
  75.8 42.8 %copy-start.15 = (bf16[1,1024,128]{2,1,0:T(8,128)(2,1)S(1)}, bf16[1,1024,128]{2,1,0:T(8,128)(2,1)}, u32[]{:S(2)}) copy-start(bf16[1,1024,128]{2,1,0:T(8,128)(2,1)} %param.31) | copy-start | bytes 786436
  119.1 4.3 %copy-start.3 = (bf16[1024,128]{1,0:T(8,128)(2,1)S(1)}, bf16[1024,128]{1,0:T(8,128)(2,1)}, u32[]{:S(2)}) copy-start(bf16[1024,128]{1,0:T(8,128)(2,1)} %param.33) | copy-start | bytes 786436
  119.1 4.5 %copy-start.4 = (bf16[128,1024]{1,0:T(8,128)(2,1)S(1)}, bf16[128,1024]{1,0:T(8,128)(2,1)}, u32[]{:S(2)}) copy-start(bf16[128,1024]{1,0:T(8,128)(2,1)} %param.35) | copy-start | bytes 786436
  119.2 4.5 %copy-start.5 = (bf16[1024,128]{1,0:T(8,128)(2,1)S(1)}, bf16[1024,128]{1,0:T(8,128)(2,1)}, u32[]{:S(2)}) copy-start(bf16[1024,128]{1,0:T(8,128)(2,1)} %param.34) | copy-start | bytes 786436
  120.0 13.3 %all-to-all-start.2 = ((bf16[4,128,2,256]{3,1,2,0:T(8,128)(2,1)}), bf16[4,128,2,256]{3,1,2,0:T(8,128)(2,1)S(1)}, u32[]{:S(2)}, u32[]{:S(2)}) async-start(bf16[4,128,2,256]{3,1,2,0:T(8,128)(2,1)} %bitcast.48), calls=%async_computation.2 | async-start | bytes 1048576 | tf_op jit(solution)/shard_map/all_to_all | solution.py:48
  123.7 44.0 %copy-start.12 = (f32[256]{0:T(256)S(1)}, f32[256]{0:T(256)}, u32[]{:S(2)}) copy-start(f32[256]{0:T(256)} %param.37) | copy-start | bytes 3076
  123.7 44.0 %copy-start.13 = (f32[256]{0:T(256)S(1)}, f32[256]{0:T(256)}, u32[]{:S(2)}) copy-start(f32[256]{0:T(256)} %param.36) | copy-start | bytes 3076
  133.3 7.6 %all-to-all-start.4 = ((bf16[4,20,256]{2,1,0:T(8,128)(2,1)}), bf16[4,20,256]{2,1,0:T(8,128)(2,1)S(1)}, u32[]{:S(2)}, u32[]{:S(2)}) async-start(bf16[4,20,256]{2,1,0:T(8,128)(2,1)} %bitcast.49), calls=%async_computation.4 | async-start | bytes 98304 | tf_op jit(solution)/shard_map/all_to_all | solution.py:48
  140.9 19.8 %all-to-all-start.3 = ((bf16[128,2,256]{2,1,0:T(2,128)(2,1)}), bf16[128,2,256]{2,1,0:T(2,128)(2,1)S(1)}, u32[]{:S(2)}, u32[]{:S(2)}) async-start(bf16[128,2,256]{2,1,0:T(2,128)(2,1)} %copy.95), calls=%async_computation.3 | async-start | bytes 262144 | tf_op jit(solution)/shard_map/all_to_all | solution.py:151
where the time goes:
time: 169 us; the launch traced here: 168 us
  blocking collectives  57.8 us (34%)
  other arithmetic  53.7 us (32%)
  waiting for transfers between devices  28.5 us (17%)
  starting transfers between devices  18.5 us (11%)
  local copies, waits for them, and re-layouts  6.46 us (4%)
  matrix products  3.03 us (2%)
    another operation x3, other arithmetic  51.4 us
    all_to_all x1, blocking collectives, body(): lax.all_to_all(parcel, 'ep', split_axis=0, concat_axis=0, tiled=True)  42.3 us
    all_to_all x1, waiting for transfers between devices, body(): lax.all_to_all(summed, 'ep', split_axis=0, concat_axis=0, tiled=True)  12.8 us
    all_to_all x2, waiting for transfers between devices, sent_and_summed(): lax.all_to_all(blocks, axis, split_axis=0, concat_axis=0, tiled=True)  12.1 us
    all_gather x1, blocking collectives, rows_first(): out, at, done = (lax.all_gather(both, axis, axis=0, tiled=True), 0, [])  9.04 us
    all_to_all x1, starting transfers between devices, body(): lax.all_to_all(summed, 'ep', split_axis=0, concat_axis=0, tiled=True)  6.93 us
    all_to_all x2, starting transfers between devices, sent_and_summed(): lax.all_to_all(blocks, axis, split_axis=0, concat_axis=0, tiled=True)  6.74 us
    all_to_all x1, blocking collectives, from_everyone(): return lax.all_to_all(copies, axis, split_axis=0, concat_axis=0, tiled=True)  6.47 us
  transfers between devices with their start and end apart: 4, of which 4 were waited for; matrix products, arithmetic and copies ran while one was open for 2% of the time, Pallas kernels for 0%

commit v1 on v0

--- a/solution.py
+++ b/solution.py
@@ -12,6 +12,11 @@
 EPSILON = 1e-05
 
 
+def gather_over(array, axis, along):
+    sent = jnp.stack([array] * lax.axis_size(axis))
+    return jnp.concatenate(lax.all_to_all(sent, axis, 0, 0), axis=along)
+
+
 def joined_along(blocks, dim):
     blocks = jnp.moveaxis(blocks, 0, dim)
     shape = blocks.shape
@@ -30,7 +35,7 @@
 def rows_first(arrays, axis, dims):
     turned = [jnp.moveaxis(a, dim, 0) for a, dim in zip(arrays, dims)]
     both = jnp.concatenate([t.reshape(len(t), -1) for t in turned], axis=1)
-    out, at, done = (lax.all_gather(both, axis, axis=0, tiled=True), 0, [])
+    out, at, done = (gather_over(both, axis, 0), 0, [])
     for t, dim in zip(turned, dims):
         piece = out[:, at : at + t[0].size].reshape(-1, *t.shape[1:])
         done.append(jnp.moveaxis(piece, 0, dim))

time: 169 us -> 167 us (0.988)
  blocking collectives: 57.8 us -> 47 us
  waiting for transfers between devices: 28.5 us -> 33.1 us
  starting transfers between devices: 18.5 us -> 21.8 us
    all_gather x1 -> x0, blocking collectives: 9.04 us -> none  [rows_first(): out, at, done = (lax.all_gather(both, axis, axis=0, tiled=True), 0, [])]
    all_to_all x0 -> x1, waiting for transfers between devices: none -> 4.49 us  [gather_over(): return jnp.concatenate(lax.all_to_all(sent, axis, 0, 0), axis=along)]
    all_to_all x0 -> x1, starting transfers between devices: none -> 3.3 us  [gather_over(): return jnp.concatenate(lax.all_to_all(sent, axis, 0, 0), axis=along)]
    all_to_all x1, blocking collectives: 42.3 us -> 40.5 us  [body(): lax.all_to_all(parcel, 'ep', split_axis=0, concat_axis=0, tiled=True)]
  transfers between devices with their start and end apart: 4 -> 5, of which waited for: 4 -> 5; matrix products, arithmetic and copies ran while one was open for 2% -> 2% of each run, Pallas kernels for 0% -> 0%
where the time goes in v1:
time: 167 us; the launch traced here: 166 us
  other arithmetic  53.7 us (32%)
  blocking collectives  47 us (28%)
  waiting for transfers between devices  33.1 us (20%)
  starting transfers between devices  21.8 us (13%)
  local copies, waits for them, and re-layouts  7.16 us (4%)
  matrix products  3.03 us (2%)
    another operation x3, other arithmetic  51.4 us
    all_to_all x1, blocking collectives, body(): lax.all_to_all(parcel, 'ep', split_axis=0, concat_axis=0, tiled=True)  40.5 us
    all_to_all x1, waiting for transfers between devices, body(): lax.all_to_all(summed, 'ep', split_axis=0, concat_axis=0, tiled=True)  12.8 us
    all_to_all x2, waiting for transfers between devices, sent_and_summed(): lax.all_to_all(blocks, axis, split_axis=0, concat_axis=0, tiled=True)  12.1 us
    all_to_all x1, starting transfers between devices, body(): lax.all_to_all(summed, 'ep', split_axis=0, concat_axis=0, tiled=True)  6.93 us
    all_to_all x2, starting transfers between devices, sent_and_summed(): lax.all_to_all(blocks, axis, split_axis=0, concat_axis=0, tiled=True)  6.74 us
    all_to_all x1, blocking collectives, from_everyone(): return lax.all_to_all(copies, axis, split_axis=0, concat_axis=0, tiled=True)  6.47 us
    all_to_all x1, starting transfers between devices, from_everyone(): return lax.all_to_all(copies, axis, split_axis=0, concat_axis=0, tiled=True)  4.83 us
  transfers between devices with their start and end apart: 5, of which 5 were waited for; matrix products, arithmetic and copies ran while one was open for 2% of the time, Pallas kernels for 0%

profile of v1, /device:TPU:1, one launch (start us, length us, event | category | flops | bytes accessed | tf_op | source)
XLA Modules:
  0.0 166.2 jit_solution(1837122258802336481)
XLA Ops:
  0.0 0.8 iota_compare_fusion.2
  0.8 1.6 copy.92
  2.6 0.4 fusion.19
  3.1 49.5 %reduce-window.6 = f32[5,2,4,8,128]{4,3,2,1,0:T(8,128)S(1)} reduce-window(f32[5,2,4,8,128]{4,3,2,1,0:T(8,128)S(1)} %reshape.123, f32[]{:T(128)} %constant.30.clone.1), window={size=1x1x1x1x128 pad=0_0x0_0x0_0x0_0x0_127}, to_apply=%region_0.1 | reduce-window | flops 5201920 | bytes 327684 | tf_op jit(solution)/shard_map/reduce-window
  52.7 1.8 %reduce-window.9 = f32[5,2,4,9]{3,2,1,0:T(4,128)S(1)} reduce-window(f32[5,2,4,8]{3,2,1,0:T(4,128)S(1)} %slice_reduce_fusion, f32[]{:T(128)} %constant.30.clone.1), window={size=1x1x1x8 pad=0_0x0_0x0_0x0_8}, to_apply=%region_1.2 | reduce-window | flops 2520 | bytes 2724 | tf_op jit(solution)/shard_map/reduce-window.1
  54.8 0.6 copy.93
  55.5 0.6 convolution_convert_fusion.3
  56.2 0.6 broadcast_in_dim.19
  56.8 4.8 %all-to-all-start = ((bf16[4,5,512]{2,1,0:T(8,128)(2,1)}), bf16[4,5,512]{2,1,0:T(8,128)(2,1)S(1)}, u32[]{:S(2)}, u32[]{:S(2)}) async-start(bf16[4,5,512]{2,1,0:T(8,128)(2,1)} %broadcast_in_dim.19), calls=%async_computation | async-start | bytes 65536 | tf_op jit(solution)/shard_map/all_to_all | solution.py:28
  61.8 0.2 convert_reduce_fusion.2
  62.2 3.7 %all-to-all-done = bf16[4,5,512]{2,1,0:T(8,128)(2,1)S(1)} async-done(((bf16[4,5,512]{2,1,0:T(8,128)(2,1)}), bf16[4,5,512]{2,1,0:T(8,128)(2,1)S(1)}, u32[]{:S(2)}, u32[]{:S(2)}) %all-to-all-start) | async-done | bytes 20512 | tf_op jit(solution)/shard_map/all_to_all | solution.py:28
  66.2 0.6 stack.2
  66.8 3.3 %all-to-all-start.1 = ((f32[4,256,22]{1,2,0:T(8,128)}), f32[4,256,22]{1,2,0:T(8,128)S(1)}, u32[]{:S(2)}, u32[]{:S(2)}) async-start(f32[4,256,22]{1,2,0:T(8,128)} %stack.2), calls=%async_computation.1 | async-start | bytes 196608 | tf_op jit(solution)/shard_map/all_to_all | solution.py:17
  70.2 4.5 %all-to-all-done.1 = f32[4,256,22]{1,2,0:T(8,128)S(1)} async-done(((f32[4,256,22]{1,2,0:T(8,128)}), f32[4,256,22]{1,2,0:T(8,128)S(1)}, u32[]{:S(2)}, u32[]{:S(2)}) %all-to-all-start.1) | async-done | bytes 90144 | tf_op jit(solution)/shard_map/all_to_all | solution.py:17
  75.1 0.3 convolution_convert_fusion.1
  75.4 0.2 reshape.130
  75.6 40.5 %all_to_all.36 = bf16[128,2,1024]{2,1,0:T(2,128)(2,1)S(1)} all-to-all(bf16[128,2,1024]{2,1,0:T(2,128)(2,1)S(1)} %reshape.130), channel_id=1, replica_groups=mesh['ep'=128,'tp'=4] {'ep'}, dimensions={0} | all-to-all | bytes 1048576 | tf_op jit(solution)/shard_map/all_to_all | solution.py:146
  116.2 0.3 fusion.7
  116.5 0.5 convolution_convert_fusion
  117.0 0.8 copy.115
  117.9 3.5 %all-to-all-start.3 = ((bf16[4,128,2,256]{3,1,2,0:T(8,128)(2,1)}), bf16[4,128,2,256]{3,1,2,0:T(8,128)(2,1)S(1)}, u32[]{:S(2)}, u32[]{:S(2)}) async-start(bf16[4,128,2,256]{3,1,2,0:T(8,128)(2,1)} %bitcast.54), calls=%async_computation.3 | async-start | bytes 1048576 | tf_op jit(solution)/shard_map/all_to_all | solution.py:53
  121.6 0.3 convolution_convert_fusion.2
  121.9 0.6 copy.117
  122.5 8.6 %all-to-all-done.3 = bf16[4,128,2,256]{3,1,2,0:T(8,128)(2,1)S(1)} async-done(((bf16[4,128,2,256]{3,1,2,0:T(8,128)(2,1)}), bf16[4,128,2,256]{3,1,2,0:T(8,128)(2,1)S(1)}, u32[]{:S(2)}, u32[]{:S(2)}) %all-to-all-start.3) | async-done | bytes 524320 | tf_op jit(solution)/shard_map/all_to_all | solution.py:53
  131.1 3.3 %all-to-all-start.5 = ((bf16[4,20,256]{2,1,0:T(8,128)(2,1)}), bf16[4,20,256]{2,1,0:T(8,128)(2,1)S(1)}, u32[]{:S(2)}, u32[]{:S(2)}) async-start(bf16[4,20,256]{2,1,0:T(8,128)(2,1)} %bitcast.56), calls=%async_computation.5 | async-start | bytes 98304 | tf_op jit(solution)/shard_map/all_to_all | solution.py:53
  134.5 0.8 copy.101
  135.3 3.5 %all-to-all-done.5 = bf16[4,20,256]{2,1,0:T(8,128)(2,1)S(1)} async-done(((bf16[4,20,256]{2,1,0:T(8,128)(2,1)}), bf16[4,20,256]{2,1,0:T(8,128)(2,1)S(1)}, u32[]{:S(2)}, u32[]{:S(2)}) %all-to-all-start.5) | async-done | bytes 40992 | tf_op jit(solution)/shard_map/all_to_all | solution.py:53
  138.8 6.9 %all-to-all-start.4 = ((bf16[128,2,256]{2,1,0:T(2,128)(2,1)}), bf16[128,2,256]{2,1,0:T(2,128)(2,1)S(1)}, u32[]{:S(2)}, u32[]{:S(2)}) async-start(bf16[128,2,256]{2,1,0:T(2,128)(2,1)} %copy.101), calls=%async_computation.4 | async-start | bytes 262144 | tf_op jit(solution)/shard_map/all_to_all | solution.py:156
  145.7 12.8 %all-to-all-done.4 = bf16[128,2,256]{2,1,0:T(2,128)(2,1)S(1)} async-done(((bf16[128,2,256]{2,1,0:T(2,128)(2,1)}), bf16[128,2,256]{2,1,0:T(2,128)(2,1)S(1)}, u32[]{:S(2)}, u32[]{:S(2)}) %all-to-all-start.4) | async-done | bytes 131104 | tf_op jit(solution)/shard_map/all_to_all | solution.py:156
  158.6 0.3 fusion.41
  159.0 6.5 %all_to_all.37 = f32[4,1,40]{2,1,0:T(1,128)S(1)} all-to-all(f32[4,1,40]{2,1,0:T(1,128)S(1)} %broadcast_in_dim.20), channel_id=1, replica_groups=mesh['ep'=128,'tp'=4] {'tp'}, dimensions={0} | all-to-all | bytes 1280 | tf_op jit(solution)/shard_map/all_to_all | solution.py:28
  165.5 0.7 add_convert_fusion.1
  (67 shorter events, 2.3 us)
Async XLA Ops:
  0.0 116.5 %copy-start = (bf16[1,128,1024]{2,1,0:T(8,128)(2,1)S(1)}, bf16[1,128,1024]{2,1,0:T(8,128)(2,1)}, u32[]{:S(2)}) copy-start(bf16[1,128,1024]{2,1,0:T(8,128)(2,1)} %param.32) | copy-start | bytes 786436
  0.8 1.6 copy-start.8
  0.8 1.7 %copy-start.16 = (f32[8]{0:T(128)S(1)}, f32[8]{0:T(128)}, u32[]{:S(2)}) copy-start(f32[8]{0:T(128)} %param.24) | copy-start | bytes 100
  2.6 52.2 %copy-start.1 = (bf16[5,1024,128]{2,1,0:T(8,128)(2,1)S(1)}, bf16[5,1024,128]{2,1,0:T(8,128)(2,1)}, u32[]{:S(2)}) copy-start(bf16[5,1024,128]{2,1,0:T(8,128)(2,1)} %param.22) | copy-start | bytes 3932164
  55.4 6.2 %copy-start.6 = (s32[20,6]{0,1:T(8,128)S(1)}, s32[20,6]{0,1:T(8,128)}, u32[]{:S(2)}) copy-start(s32[20,6]{0,1:T(8,128)} %param.28) | copy-start | bytes 1444
  55.4 10.5 %copy-start.2 = (bf16[512,256]{1,0:T(8,128)(2,1)S(1)}, bf16[512,256]{1,0:T(8,128)(2,1)}, u32[]{:S(2)}) copy-start(bf16[512,256]{1,0:T(8,128)(2,1)} %param.25) | copy-start | bytes 786436
  55.4 10.5 %copy-start.7 = (bf16[20,256]{1,0:T(8,128)(2,1)S(1)}, bf16[20,256]{1,0:T(8,128)(2,1)}, u32[]{:S(2)}) copy-start(bf16[20,256]{1,0:T(8,128)(2,1)} %param.19) | copy-start | bytes 30724
  55.5 10.7 %copy-start.10 = (f32[256]{0:T(256)S(1)}, f32[256]{0:T(256)}, u32[]{:S(2)}) copy-start(f32[256]{0:T(256)} %param.27) | copy-start | bytes 3076
  55.5 10.7 %copy-start.11 = (f32[256]{0:T(256)S(1)}, f32[256]{0:T(256)}, u32[]{:S(2)}) copy-start(f32[256]{0:T(256)} %param.26) | copy-start | bytes 3076
  55.5 14.6 %copy-start.9 = (f32[20,6]{0,1:T(8,128)S(1)}, f32[20,6]{0,1:T(8,128)}, u32[]{:S(2)}) copy-start(f32[20,6]{0,1:T(8,128)} %param.29) | copy-start | bytes 1444
  56.8 9.1 %all-to-all-start = ((bf16[4,5,512]{2,1,0:T(8,128)(2,1)}), bf16[4,5,512]{2,1,0:T(8,128)(2,1)S(1)}, u32[]{:S(2)}, u32[]{:S(2)}) async-start(bf16[4,5,512]{2,1,0:T(8,128)(2,1)} %broadcast_in_dim.19), calls=%async_computation | async-start | bytes 65536 | tf_op jit(solution)/shard_map/all_to_all | solution.py:28
  66.8 7.9 %all-to-all-start.1 = ((f32[4,256,22]{1,2,0:T(8,128)}), f32[4,256,22]{1,2,0:T(8,128)S(1)}, u32[]{:S(2)}, u32[]{:S(2)}) async-start(f32[4,256,22]{1,2,0:T(8,128)} %stack.2), calls=%async_computation.1 | async-start | bytes 196608 | tf_op jit(solution)/shard_map/all_to_all | solution.py:17
  75.1 41.1 %copy-start.14 = (bf16[1,1024,128]{2,1,0:T(8,128)(2,1)S(1)}, bf16[1,1024,128]{2,1,0:T(8,128)(2,1)}, u32[]{:S(2)}) copy-start(bf16[1,1024,128]{2,1,0:T(8,128)(2,1)} %param.30) | copy-start | bytes 786436
  75.4 41.1 %copy-start.15 = (bf16[1,1024,128]{2,1,0:T(8,128)(2,1)S(1)}, bf16[1,1024,128]{2,1,0:T(8,128)(2,1)}, u32[]{:S(2)}) copy-start(bf16[1,1024,128]{2,1,0:T(8,128)(2,1)} %param.31) | copy-start | bytes 786436
  117.0 4.3 %copy-start.3 = (bf16[1024,128]{1,0:T(8,128)(2,1)S(1)}, bf16[1024,128]{1,0:T(8,128)(2,1)}, u32[]{:S(2)}) copy-start(bf16[1024,128]{1,0:T(8,128)(2,1)} %param.33) | copy-start | bytes 786436
  117.0 4.5 %copy-start.4 = (bf16[128,1024]{1,0:T(8,128)(2,1)S(1)}, bf16[128,1024]{1,0:T(8,128)(2,1)}, u32[]{:S(2)}) copy-start(bf16[128,1024]{1,0:T(8,128)(2,1)} %param.35) | copy-start | bytes 786436
  117.0 4.5 %copy-start.5 = (bf16[1024,128]{1,0:T(8,128)(2,1)S(1)}, bf16[1024,128]{1,0:T(8,128)(2,1)}, u32[]{:S(2)}) copy-start(bf16[1024,128]{1,0:T(8,128)(2,1)} %param.34) | copy-start | bytes 786436
  117.9 13.3 %all-to-all-start.3 = ((bf16[4,128,2,256]{3,1,2,0:T(8,128)(2,1)}), bf16[4,128,2,256]{3,1,2,0:T(8,128)(2,1)S(1)}, u32[]{:S(2)}, u32[]{:S(2)}) async-start(bf16[4,128,2,256]{3,1,2,0:T(8,128)(2,1)} %bitcast.54), calls=%async_computation.3 | async-start | bytes 1048576 | tf_op jit(solution)/shard_map/all_to_all | solution.py:53
  121.5 44.0 %copy-start.12 = (f32[256]{0:T(256)S(1)}, f32[256]{0:T(256)}, u32[]{:S(2)}) copy-start(f32[256]{0:T(256)} %param.37) | copy-start | bytes 3076
  121.5 44.0 %copy-start.13 = (f32[256]{0:T(256)S(1)}, f32[256]{0:T(256)}, u32[]{:S(2)}) copy-start(f32[256]{0:T(256)} %param.36) | copy-start | bytes 3076
  131.1 7.6 %all-to-all-start.5 = ((bf16[4,20,256]{2,1,0:T(8,128)(2,1)}), bf16[4,20,256]{2,1,0:T(8,128)(2,1)S(1)}, u32[]{:S(2)}, u32[]{:S(2)}) async-start(bf16[4,20,256]{2,1,0:T(8,128)(2,1)} %bitcast.56), calls=%async_computation.5 | async-start | bytes 98304 | tf_op jit(solution)/shard_map/all_to_all | solution.py:53
  138.8 19.8 %all-to-all-start.4 = ((bf16[128,2,256]{2,1,0:T(2,128)(2,1)}), bf16[128,2,256]{2,1,0:T(2,128)(2,1)S(1)}, u32[]{:S(2)}, u32[]{:S(2)}) async-start(bf16[128,2,256]{2,1,0:T(2,128)(2,1)} %copy.101), calls=%async_computation.4 | async-start | bytes 262144 | tf_op jit(solution)/shard_map/all_to_all | solution.py:156
